TPU v7x, 32 devices: a whole 2x2x4 slice. The times are simulated.
32 devices in a mesh: ep: 16 (over z, y, x), tp: 2 (over core).
Axes of the slice: x: 2, y: 2, z: 4, core: 2. Of those that a mesh axis runs over, the one named last changes fastest.
Arguments:
- tokens: bfloat16 [512, 4096], P('ep'), may hold values from -6 to 6
- norm_gain: float32 [4096], replicated, may hold values from 0.1 to 1.9
- expert_ids: int32 [512, 2], P('ep'), may hold values from 0 to 15, all different within a row; in each aligned block of 32 rows (0 to 31, 32 to 63, ...) at most 8 rows name the same one
- gates: float32 [512, 2], P('ep'), may hold values from 0.1 to 1
- w_gate: bfloat16 [16, 4096, 768], P('ep', None, 'tp'), may hold values from -0.09375 to 0.09375
- w_up: bfloat16 [16, 4096, 768], P('ep', None, 'tp'), may hold values from -0.09375 to 0.09375
- w_down: bfloat16 [16, 768, 4096], P('ep', 'tp'), may hold values from -1 to 1, as said below
- post_gain: float32 [4096], P('tp'), may hold values from 0.1 to 1.9
Outputs:
- mixed: bfloat16 [512, 4096], P('ep', 'tp')
Inputs may be any that keep to these rules, and one draw needn't show every extreme that they name: `expert_ids`: each row names 2 different experts; among the 32 rows of one device (aligned blocks) no expert is named more than 8 times. `w_down`: entries of the down projections lie between -1 and 1, both reached.
All inputs are finite; a program needn't handle non-finite values.
Results may differ from a plain program's by a relative error of at most 0.015.
Values may be sent and summed in bfloat16 or wider, within the bound.
A program may use at most 64 MiB of HBM per device.

v0:
```python
import jax
import jax.numpy as jnp
from jax import lax
from jax.sharding import PartitionSpec as P

SLOTS = 8


RMS_EPS = 1e-06


def shards(tokens, norm_gain, expert_ids, gates, w_gate, w_up, w_down, post_gain):
    tok_dev, features = tokens.shape
    top_count = expert_ids.shape[1]
    experts = lax.axis_size("ep")
    capacity = experts * SLOTS
    floats = tokens.astype(jnp.float32)
    inverse = lax.rsqrt(jnp.mean(floats * floats, axis=-1, keepdims=True) + RMS_EPS)
    normed = (floats * inverse * norm_gain).astype(jnp.bfloat16)
    flat_ids = expert_ids.reshape(-1)
    onehot = (flat_ids[:, None] == jnp.arange(experts, dtype=jnp.int32)[None, :]).astype(jnp.int32)
    earlier = jnp.cumsum(onehot, axis=0) - onehot
    slot_index = jnp.sum(earlier * onehot, axis=1).astype(jnp.int32)
    position = (flat_ids * SLOTS + slot_index).astype(jnp.int32)

    def expert(picked_rows):
        gate_proj = jnp.dot(picked_rows, w_gate[0], preferred_element_type=jnp.float32)
        up_proj = jnp.dot(picked_rows, w_up[0], preferred_element_type=jnp.float32)
        hidden = (jax.nn.silu(gate_proj) * up_proj).astype(jnp.bfloat16)
        partial_value = jnp.dot(hidden, w_down[0], preferred_element_type=jnp.float32)
        return (
            lax.psum_scatter(
                partial_value.astype(jnp.bfloat16), "tp", scatter_dimension=1, tiled=True
            )
            .astype(jnp.float32)
            .astype(jnp.bfloat16)
        )

    dispatch = position[:, None] == jnp.arange(capacity, dtype=jnp.int32)[None, :]
    route_rows = jnp.repeat(normed, top_count, axis=0)
    send_rows = jnp.dot(
        dispatch.astype(jnp.bfloat16).T, route_rows, preferred_element_type=jnp.float32
    ).astype(jnp.bfloat16)
    received = lax.all_to_all(send_rows, "ep", split_axis=0, concat_axis=0, tiled=True)
    own_rows = expert(received)
    returned = lax.all_to_all(own_rows, "ep", split_axis=0, concat_axis=0, tiled=True)
    combine_rows = dispatch.astype(jnp.float32) * gates.reshape(-1)[:, None]
    combine_rows = jnp.sum(combine_rows.reshape(tok_dev, top_count, capacity), axis=1)
    combined = jnp.dot(combine_rows, returned.astype(jnp.float32), precision=lax.Precision.HIGHEST)
    combined_low = combined.astype(jnp.bfloat16).astype(jnp.float32)
    squared = jnp.sum(combined_low * combined_low, axis=1)
    totals = lax.psum(squared, "tp")
    inverse_rms = lax.rsqrt(totals / features + RMS_EPS)
    return (combined_low * inverse_rms[:, None] * post_gain).astype(jnp.bfloat16)


def solution(mesh):
    in_specs = (
        P("ep", None),
        P(),
        P("ep", None),
        P("ep", None),
        P("ep", None, "tp"),
        P("ep", None, "tp"),
        P("ep", "tp", None),
        P("tp"),
    )
    out_specs = P("ep", "tp")
    return jax.shard_map(shards, mesh=mesh, in_specs=in_specs, out_specs=out_specs, check_vma=False)
```

profile of v0, /device:TPU:0, one launch (start us, length us, event | category | flops | bytes accessed | tf_op | source)
XLA Modules:
  0.0 97.0 jit_solution(1257142370337697468)
XLA Ops:
  6.5 0.0 copy-start
  6.5 0.0 reduce-scatter.2.cloned.1.call-start
  6.5 0.9 copy.21
  7.4 0.1 eq.35
  7.6 0.1 fusion.28
  7.6 0.1 reduce_window_sum.11
  7.7 0.2 select_reduce_fusion.1
  7.9 1.1 %fusion.18 = f32[32]{0:T(128)S(1)} fusion(bf16[32,4096]{1,0:T(8,128)(2,1)} %param.8), kind=kLoop, calls=%fused_computation.16 | loop fusion | flops 393184 | bytes 262272 | tf_op jit(solution)/shard_map/reduce_sum | solution.py:18
  9.0 1.1 %fusion.20 = bf16[32,4096]{1,0:T(8,128)(2,1)S(1)} fusion(bf16[32,4096]{1,0:T(8,128)(2,1)} %param.8, f32[4096]{0:T(1024)} %param.9, f32[32]{0:T(128)S(1)} %add_rsqrt_fusion.1), kind=kLoop, calls=%fused_computation.18 | loop fusion | flops 524288 | bytes 540800 | tf_op jit(solution)/shard_map/convert_element_type | solution.py:19
  10.1 1.3 %broadcast_in_dim.2 = bf16[32,2,4096]{2,1,0:T(2,128)(2,1)} broadcast(bf16[32,4096]{1,0:T(8,128)(2,1)S(1)} %fusion.20), dimensions={0,2} | broadcast | bytes 786432 | tf_op jit(solution)/shard_map/broadcast_in_dim | solution.py:40
  11.4 2.0 %reshape.44 = bf16[64,4096]{1,0:T(8,128)(2,1)} reshape(bf16[32,2,4096]{2,1,0:T(2,128)(2,1)} %broadcast_in_dim.2) | data formatting | bytes 1048576 | tf_op jit(solution)/shard_map/reshape | solution.py:40
  13.5 1.7 %fusion = bf16[16,8,4096]{2,1,0:T(8,128)(2,1)S(1)} fusion(bf16[64,4096]{1,0:T(8,128)(2,1)} %reshape.44, s32[64]{0:T(128)S(1)} %multiply_add_fusion.1), kind=kOutput, calls=%fused_computation.2 | convolution fusion | flops 67641344 | bytes 1573120 | tf_op jit(solution)/shard_map/dot_general | solution.py:41
  15.2 34.5 %all_to_all.24 = bf16[16,8,4096]{2,1,0:T(8,128)(2,1)S(1)} all-to-all(bf16[16,8,4096]{2,1,0:T(8,128)(2,1)S(1)} %fusion), channel_id=1, replica_groups=mesh['ep'=16,'tp'=2] {'ep'}, dimensions={0} | all-to-all | bytes 2097152 | tf_op jit(solution)/shard_map/all_to_all | solution.py:44
  49.7 1.0 %copy-done.1 = bf16[16,8,4096]{2,1,0:T(8,128)(2,1)} copy-done((bf16[16,8,4096]{2,1,0:T(8,128)(2,1)}, bf16[16,8,4096]{2,1,0:T(8,128)(2,1)S(1)}, u32[]{:S(2)}) %copy-start.1) | copy-done | bytes 1048600
  50.8 0.0 copy-done.2
  50.8 0.7 fusion.4
  51.5 0.0 copy-done
  51.5 0.0 copy-start.4
  51.5 0.0 copy-start.5
  51.5 0.0 copy-start.3
  51.5 4.6 %convolution_convert_fusion = bf16[128,4096]{1,0:T(8,128)(2,1)} fusion(bf16[1,384,4096]{2,1,0:T(8,128)(2,1)S(1)} %copy-done, bf16[1,4096,384]{2,1,0:T(8,128)(2,1)} %param.13, bf16[16,8,4096]{2,1,0:T(8,128)(2,1)} %copy-done.1, f32[128,384]{1,0:T(8,128)S(1)} %fusion.4), kind=kOutput, calls=%fused_computation | convolution fusion | flops 806125568 | bytes 8585216 | tf_op jit(solution)/shard_map/dot_general | solution.py:30
  56.1 0.0 reduce-scatter.2.cloned.1.call-update
  56.2 6.8 %reduce-scatter.2.cloned.1.call-done = bf16[128,2048]{1,0:T(8,128)(2,1)} async-done(((bf16[128,4096]{1,0:T(8,128)(2,1)}), bf16[128,2048]{1,0:T(8,128)(2,1)}) %reduce-scatter.2.cloned.1.call-update) | async-done | bytes 524304 | tf_op jit(solution)/shard_map/reduce_scatter | solution.py:32
  63.0 6.8 %all-to-all-start.1 = ((bf16[16,8,2048]{2,1,0:T(8,128)(2,1)}), bf16[16,8,2048]{2,1,0:T(8,128)(2,1)}, u32[]{:S(2)}, u32[]{:S(2)}) async-start(bf16[16,8,2048]{2,1,0:T(8,128)(2,1)} %bitcast.31), calls=%async_computation.2 | async-start | bytes 1048576 | tf_op jit(solution)/shard_map/all_to_all | solution.py:46
  69.9 0.1 reduce_sum.39
  70.0 0.1 copy.22
  70.0 0.0 copy-done.5
  70.1 0.1 select_reduce_fusion
  70.1 15.3 %all-to-all-done.1 = bf16[16,8,2048]{2,1,0:T(8,128)(2,1)} async-done(((bf16[16,8,2048]{2,1,0:T(8,128)(2,1)}), bf16[16,8,2048]{2,1,0:T(8,128)(2,1)}, u32[]{:S(2)}, u32[]{:S(2)}) %all-to-all-start.1) | async-done | bytes 524320 | tf_op jit(solution)/shard_map/all_to_all | solution.py:46
  85.5 1.5 %multiply_reduce_fusion = (f32[32]{0:T(128)S(1)}, f32[32,2048]{1,0:T(8,128)S(1)}) fusion(f32[32,128]{1,0:T(8,128)S(1)} %select_reduce_fusion, bf16[16,8,2048]{2,1,0:T(8,128)(2,1)} %all-to-all-done.1), kind=kOutput, calls=%fused_computation.21 | convolution fusion | flops 100925408 | bytes 802944 | tf_op jit(solution)/shard_map/dot_general | solution.py:49
  86.9 2.5 %psum.7 = f32[32]{0:T(128)S(1)} all-reduce(f32[32]{0:T(128)S(1)} %get-tuple-element.5), channel_id=1, replica_groups=mesh['ep'=16,'tp'=2] {'tp'}, use_global_device_ids=true, to_apply=%region_6.7 | all-reduce | flops 32 | bytes 256 | tf_op jit(solution)/shard_map/psum | solution.py:52
  89.4 0.8 multiply_convert_fusion
  (8 shorter events, 0.0 us)
Async XLA Ops:
  6.5 45.0 %copy-start = (bf16[1,384,4096]{2,1,0:T(8,128)(2,1)S(1)}, bf16[1,384,4096]{2,1,0:T(8,128)(2,1)}, u32[]{:S(2)}) copy-start(bf16[1,384,4096]{2,1,0:T(8,128)(2,1)} %param.14) | copy-start | bytes 9437188
  6.5 56.5 %reduce-scatter.2.cloned.1.call-start = ((), (), s32[]{:S(2)}) async-start(), calls=%async_computation.3 | async-start | bytes 1572864 | tf_op jit(solution)/shard_map/reduce_scatter | solution.py:32
  13.5 37.3 %copy-start.2 = (bf16[1,4096,384]{2,1,0:T(8,128)(2,1)S(1)}, bf16[1,4096,384]{2,1,0:T(8,128)(2,1)}, u32[]{:S(2)}) copy-start(bf16[1,4096,384]{2,1,0:T(8,128)(2,1)} %param.12) | copy-start | bytes 9437188
  49.7 1.0 %copy-start.1 = (bf16[16,8,4096]{2,1,0:T(8,128)(2,1)}, bf16[16,8,4096]{2,1,0:T(8,128)(2,1)S(1)}, u32[]{:S(2)}) copy-start(bf16[16,8,4096]{2,1,0:T(8,128)(2,1)S(1)} %all_to_all.24) | copy-start | bytes 3145732
  51.5 18.5 %copy-start.4 = (s32[32,2]{0,1:T(2,128)S(1)}, s32[32,2]{0,1:T(2,128)}, u32[]{:S(2)}) copy-start(s32[32,2]{0,1:T(2,128)} %param.10) | copy-start | bytes 772
  51.5 18.5 %copy-start.5 = (f32[32,2]{0,1:T(2,128)S(1)}, f32[32,2]{0,1:T(2,128)}, u32[]{:S(2)}) copy-start(f32[32,2]{0,1:T(2,128)} %param.11) | copy-start | bytes 772
  51.5 37.9 %copy-start.3 = (f32[2048]{0:T(1024)S(1)}, f32[2048]{0:T(1024)}, u32[]{:S(2)}) copy-start(f32[2048]{0:T(1024)} %param.15) | copy-start | bytes 24580
  63.0 22.5 %all-to-all-start.1 = ((bf16[16,8,2048]{2,1,0:T(8,128)(2,1)}), bf16[16,8,2048]{2,1,0:T(8,128)(2,1)}, u32[]{:S(2)}, u32[]{:S(2)}) async-start(bf16[16,8,2048]{2,1,0:T(8,128)(2,1)} %bitcast.31), calls=%async_computation.2 | async-start | bytes 1048576 | tf_op jit(solution)/shard_map/all_to_all | solution.py:46
Sparse Core Ops, SparseCore 0:
  56.3 6.6 reduce-scatter.1
where the time goes:
time: 97.4 us; the launch traced here: 97 us
  blocking collectives  37 us (38%)
  waiting for transfers between devices  22.2 us (23%)
  between operations  13.5 us (14%)
  matrix products  8.51 us (9%)
  starting transfers between devices  6.85 us (7%)
  local copies, waits for them, and re-layouts  5.57 us (6%)
  other arithmetic  3.42 us (4%)
    all_to_all x1, blocking collectives, shards(): lax.all_to_all(send_rows, 'ep', split_axis=0, concat_axis=0, tiled=True)  34.5 us
    all_to_all x1, waiting for transfers between devices, shards(): lax.all_to_all(own_rows, 'ep', split_axis=0, concat_axis=0, tiled=True)  15.3 us
    all_to_all x1, starting transfers between devices, shards(): lax.all_to_all(own_rows, 'ep', split_axis=0, concat_axis=0, tiled=True)  6.85 us
    reduce_scatter x1, waiting for transfers between devices, expert(): lax.psum_scatter(partial_value.astype(jnp.bfloat16), 'tp', scatter_dimens...  6.84 us
    dot_general x1, matrix products, expert(): jnp.dot(hidden, w_down[0], preferred_element_type=jnp.float32)  4.59 us
    psum x1, blocking collectives, shards(): totals = lax.psum(squared, 'tp')  2.47 us
    reshape x1, local copies, waits for them, and re-layouts, shards(): route_rows = jnp.repeat(normed, top_count, axis=0)  2.05 us
    unnamed x13, local copies, waits for them, and re-layouts  1.97 us
  transfers between devices with their start and end apart: 2, of which 2 were waited for; matrix products, arithmetic and copies ran while one was open for 0% of the time, Pallas kernels for 0%

commit v1 on v0

v1 whole, which is shorter than its diff:
```python
import functools

import jax
import jax.numpy as jnp
from jax import lax
from jax.experimental import pallas as pl
from jax.experimental.pallas import tpu as pltpu
from jax.sharding import PartitionSpec as P

SLOTS = 8
RMS_EPS = 1e-06
MESH = pl.DeviceIdType.MESH
F32 = jnp.float32
BF16 = jnp.bfloat16


def kernel(
    n, n_tp,
    tok_ref, gain_ref, ids_ref, gates_ref, post_ref, wg_ref, wu_ref, wd_ref,
    out_ref,
    send_buf, x_buf, wgu, wdn, h_buf, o_buf, ret_buf, stat_buf,
    w_sem, wx_send, wx_recv, d_send, d_recv, f_send, f_recv,
    h_send, h_recv, r_send, r_recv, s_send, s_recv,
):
    me = lax.axis_index("ep")
    core = lax.axis_index("tp")
    other = 1 - core
    rows, features = tok_ref.shape
    half = features // n_tp
    part = wg_ref.shape[2]
    cap = n * SLOTS

    def step(i):
        return 1 + lax.rem(n // 2 - 1 + i, n - 1)

    barrier = pltpu.get_barrier_semaphore()

    def greet(k, _):
        pl.semaphore_signal(barrier, inc=1, device_id={"ep": lax.rem(me + k, n)}, device_id_type=MESH)
        return 0

    lax.fori_loop(1, n, greet, 0)
    pl.semaphore_signal(barrier, inc=1, device_id={"tp": other}, device_id_type=MESH)

    own_cols = pl.ds(pl.multiple_of(core * half, half), half)
    other_cols = pl.ds(pl.multiple_of(other * half, half), half)
    own_part = pl.ds(pl.multiple_of(core * part, part), part)
    copies = [
        pltpu.make_async_copy(wg_ref.at[0], wgu.at[:, pl.ds(0, part)], w_sem.at[0]),
        pltpu.make_async_copy(wu_ref.at[0], wgu.at[:, pl.ds(part, part)], w_sem.at[1]),
        pltpu.make_async_copy(wd_ref.at[0, :, own_cols], wdn.at[own_part], w_sem.at[2]),
    ]
    for copy in copies:
        copy.start()

    ids = ids_ref[...]
    lanes = lax.broadcasted_iota(jnp.int32, (rows, n), 1)
    before = (
        lax.broadcasted_iota(jnp.int32, (rows, rows), 1)
        < lax.broadcasted_iota(jnp.int32, (rows, rows), 0)
    ).astype(BF16)
    slots = lax.broadcasted_iota(jnp.int32, (rows, cap), 1)
    count = jnp.zeros((1, n), F32)
    picks = []
    for j in range(ids.shape[1]):
        hot = (ids[:, j:j + 1] == lanes).astype(F32)
        earlier = jnp.dot(before, hot.astype(BF16), preferred_element_type=F32) + count
        slot = jnp.sum(earlier * hot, axis=1, keepdims=True).astype(jnp.int32)
        count = count + jnp.sum(hot, axis=0, keepdims=True)
        picks.append((slots == ids[:, j:j + 1] * SLOTS + slot).astype(F32))

    floats = tok_ref[...].astype(F32)
    inverse = lax.rsqrt(jnp.mean(floats * floats, axis=1, keepdims=True) + RMS_EPS)
    mine = tok_ref[:, own_cols].astype(F32)
    normed = (mine * inverse * gain_ref[:, own_cols]).astype(BF16)
    dispatch = functools.reduce(lambda a, b: a + b, picks).T.astype(BF16)
    sent = jnp.dot(dispatch, normed, preferred_element_type=F32)
    send_buf[...] = sent.reshape(n, SLOTS, half).astype(BF16)

    pl.semaphore_wait(barrier, n)

    def to_expert(i):
        peer = lax.rem(me + step(i), n)
        return pltpu.make_async_remote_copy(
            src_ref=send_buf.at[peer], dst_ref=x_buf.at[me, core],
            send_sem=d_send.at[peer], recv_sem=d_recv.at[me],
            device_id={"ep": peer}, device_id_type=MESH)

    def from_token(i):
        peer = lax.rem(me + n - step(i), n)
        return peer, pltpu.make_async_remote_copy(
            src_ref=send_buf.at[peer], dst_ref=x_buf.at[peer, core],
            send_sem=d_send.at[peer], recv_sem=d_recv.at[peer],
            device_id={"ep": peer}, device_id_type=MESH)

    def forward(src, block):
        return pltpu.make_async_remote_copy(
            src_ref=src, dst_ref=x_buf.at[block, core],
            send_sem=f_send.at[block], recv_sem=f_recv.at[block],
            device_id={"tp": other}, device_id_type=MESH)

    def start_send(i, _):
        to_expert(i).start()
        return 0

    lax.fori_loop(0, n - 1, start_send, 0)
    own_x = pltpu.make_async_copy(send_buf.at[me], x_buf.at[me, core], w_sem.at[3])
    own_x.start()
    forward(send_buf.at[me], me).start()
    down_x = pltpu.make_async_remote_copy(
        src_ref=wd_ref.at[0, :, other_cols], dst_ref=wdn.at[own_part],
        send_sem=wx_send, recv_sem=wx_recv,
        device_id={"tp": other}, device_id_type=MESH)
    down_x.start()

    def pass_on(i, _):
        peer, copy = from_token(i)
        copy.wait_recv()
        forward(x_buf.at[peer, core], peer).start()
        return 0

    lax.fori_loop(0, n - 1, pass_on, 0)
    own_x.wait()

    def arrived(i, _):
        forward(x_buf.at[i, core], i).wait_recv()
        return 0

    lax.fori_loop(0, n, arrived, 0)
    for copy in copies:
        copy.wait()

    acc = jnp.zeros((cap, 2 * part), F32)
    for side in range(n_tp):
        x = x_buf[:, side].astype(F32).reshape(cap, half).astype(BF16)
        acc = acc + jnp.dot(x, wgu[side * half:(side + 1) * half], preferred_element_type=F32)
    gate = acc[:, :part]
    up = acc[:, part:]
    hidden = (gate / (1.0 + jnp.exp(-gate)) * up).astype(BF16)
    h_buf[:, own_part] = hidden
    hx = pltpu.make_async_remote_copy(
        src_ref=h_buf.at[:, own_part], dst_ref=h_buf.at[:, own_part],
        send_sem=h_send, recv_sem=h_recv,
        device_id={"tp": other}, device_id_type=MESH)
    hx.start()
    down_x.wait()
    hx.wait()

    result = jnp.dot(h_buf[...], wdn[...], preferred_element_type=F32)
    o_buf[...] = result.reshape(n, SLOTS, half).astype(BF16)

    def give_back(i):
        peer = lax.rem(me + step(i), n)
        return pltpu.make_async_remote_copy(
            src_ref=o_buf.at[peer], dst_ref=ret_buf.at[me],
            send_sem=r_send.at[peer], recv_sem=r_recv.at[me],
            device_id={"ep": peer}, device_id_type=MESH)

    def take_back(i):
        peer = lax.rem(me + n - step(i), n)
        return pltpu.make_async_remote_copy(
            src_ref=o_buf.at[peer], dst_ref=ret_buf.at[peer],
            send_sem=r_send.at[peer], recv_sem=r_recv.at[peer],
            device_id={"ep": peer}, device_id_type=MESH)

    def start_back(i, _):
        give_back(i).start()
        return 0

    lax.fori_loop(0, n - 1, start_back, 0)
    own_r = pltpu.make_async_copy(o_buf.at[me], ret_buf.at[me], w_sem.at[4])
    own_r.start()

    def sent_all(i, _):
        to_expert(i).wait_send()
        return 0

    lax.fori_loop(0, n - 1, sent_all, 0)

    def passed_all(i, _):
        forward(x_buf.at[i, core], i).wait_send()
        return 0

    lax.fori_loop(0, n, passed_all, 0)

    def back(i, _):
        take_back(i).wait_recv()
        return 0

    lax.fori_loop(0, n - 1, back, 0)
    own_r.wait()

    returned = ret_buf[...].astype(F32).reshape(cap, half).astype(BF16)
    combined = jnp.zeros((rows, half), F32)
    for j, pick in enumerate(picks):
        row = jnp.dot(pick.astype(BF16), returned, preferred_element_type=F32)
        combined = combined + gates_ref[:, j:j + 1] * row
    low = combined.astype(BF16).astype(F32)
    squared = jnp.sum(low * low, axis=1, keepdims=True)
    stat_buf[0] = jnp.broadcast_to(squared, (rows, 128))
    sx = pltpu.make_async_remote_copy(
        src_ref=stat_buf.at[0], dst_ref=stat_buf.at[1],
        send_sem=s_send, recv_sem=s_recv,
        device_id={"tp": other}, device_id_type=MESH)
    sx.start()

    def back_sent(i, _):
        give_back(i).wait_send()
        return 0

    lax.fori_loop(0, n - 1, back_sent, 0)
    sx.wait()
    total = squared + stat_buf[1][:, 0:1]
    scale = lax.rsqrt(total / features + RMS_EPS)
    out_ref[...] = (low * scale * post_ref[...]).astype(BF16)


def shards(n, n_tp, tokens, norm_gain, expert_ids, gates, w_gate, w_up, w_down, post_gain):
    rows, features = tokens.shape
    half = features // n_tp
    part = w_gate.shape[2]
    vmem = pl.BlockSpec(memory_space=pltpu.VMEM)
    hbm = pl.BlockSpec(memory_space=pl.ANY)
    dma = pltpu.SemaphoreType.DMA
    cap = n * SLOTS
    return pl.pallas_call(
        functools.partial(kernel, n, n_tp),
        out_shape=jax.ShapeDtypeStruct((rows, half), BF16),
        in_specs=[vmem] * 5 + [hbm] * 3,
        out_specs=vmem,
        scratch_shapes=[
            pltpu.VMEM((n, SLOTS, half), BF16),
            pltpu.VMEM((n, n_tp, SLOTS, half), BF16),
            pltpu.VMEM((features, 2 * part), BF16),
            pltpu.VMEM((n_tp * part, half), BF16),
            pltpu.VMEM((cap, n_tp * part), BF16),
            pltpu.VMEM((n, SLOTS, half), BF16),
            pltpu.VMEM((n, SLOTS, half), BF16),
            pltpu.VMEM((2, rows, 128), F32),
            dma((5,)), dma, dma,
            dma((n,)), dma((n,)), dma((n,)), dma((n,)),
            dma, dma, dma((n,)), dma((n,)), dma, dma,
        ],
        compiler_params=pltpu.CompilerParams(
            collective_id=0, has_side_effects=True, vmem_limit_bytes=60 * 1024 * 1024
        ),
    )(
        tokens, norm_gain.reshape(1, -1), expert_ids, gates, post_gain.reshape(1, -1),
        w_gate, w_up, w_down,
    )


def solution(mesh):
    in_specs = (
        P("ep", None),
        P(),
        P("ep", None),
        P("ep", None),
        P("ep", None, "tp"),
        P("ep", None, "tp"),
        P("ep", "tp", None),
        P("tp"),
    )
    body = functools.partial(shards, mesh.shape["ep"], mesh.shape["tp"])
    return jax.shard_map(body, mesh=mesh, in_specs=in_specs, out_specs=P("ep", "tp"), check_vma=False)
```

time: 97.4 us -> 46.4 us (0.48)
  Pallas kernels: 0 us -> 41.9 us
  blocking collectives: 37 us -> 0 us
  waiting for transfers between devices: 22.2 us -> 0 us
  between operations: 13.5 us -> 0.01 us
  matrix products: 8.51 us -> 0 us
  starting transfers between devices: 6.85 us -> 0 us
  other arithmetic: 3.42 us -> 0 us
  local copies, waits for them, and re-layouts: 5.57 us -> 4.29 us
    pallas_call x0 -> x1, Pallas kernels: none -> 41.9 us  [shards(): pl.pallas_call(functools.partial(kernel, n, n_tp), out_shape=jax.ShapeDty...]
    all_to_all x1 -> x0, blocking collectives: 34.5 us -> none  [shards(): lax.all_to_all(send_rows, 'ep', split_axis=0, concat_axis=0, tiled=True)]
    all_to_all x1 -> x0, waiting for transfers between devices: 15.3 us -> none  [shards(): lax.all_to_all(own_rows, 'ep', split_axis=0, concat_axis=0, tiled=True)]
    dot_general x4 -> x0, matrix products: 8.51 us -> none  [the longest x1 4.59 us: expert(): jnp.dot(hidden, w_down[0], preferred_element_type=jnp.float32)]
    all_to_all x1 -> x0, starting transfers between devices: 6.85 us -> none  [shards(): lax.all_to_all(own_rows, 'ep', split_axis=0, concat_axis=0, tiled=True)]
    reduce_scatter x1 -> x0, waiting for transfers between devices: 6.84 us -> none  [expert(): lax.psum_scatter(partial_value.astype(jnp.bfloat16), 'tp', scatter_dimens...]
    psum x1 -> x0, blocking collectives: 2.47 us -> none  [shards(): totals = lax.psum(squared, 'tp')]
    unnamed x13 -> x3, local copies, waits for them, and re-layouts: 1.97 us -> 4.29 us
  transfers between devices with their start and end apart: 2 -> 0, of which waited for: 2 -> 0; matrix products, arithmetic and copies ran while one was open for 0% -> 0% of each run, Pallas kernels for 0% -> 0%
where the time goes in v1:
time: 46.4 us; the launch traced here: 46.2 us
  Pallas kernels  41.9 us (90%)
  local copies, waits for them, and re-layouts  4.29 us (9%)
    pallas_call x1, Pallas kernels, shards(): pl.pallas_call(functools.partial(kernel, n, n_tp), out_shape=jax.ShapeDty...  41.9 us
    unnamed x3, local copies, waits for them, and re-layouts  4.29 us

profile of v1, /device:TPU:0, one launch (start us, length us, event | category | flops | bytes accessed | tf_op | source)
XLA Modules:
  0.0 46.2 jit_solution(7628526600250510057)
XLA Ops:
  0.0 1.4 %copy.9.ids_ref = s32[32,2]{1,0:T(8,128)} copy(s32[32,2]{0,1:T(2,128)} %param.10) | data formatting | bytes 512 | tf_op args[2]
  1.4 1.4 %copy.10.gates_ref = f32[32,2]{1,0:T(8,128)} copy(f32[32,2]{0,1:T(2,128)} %param.11) | data formatting | bytes 512 | tf_op args[3]
  2.7 41.9 %shard_map.82 = bf16[32,2048]{1,0:T(8,128)(2,1)} custom-call(bf16[32,4096]{1,0:T(8,128)(2,1)} %tok_ref.1, f32[1,4096]{1,0:T(1,128)} %bitcast.2, s32[32,2]{1,0:T(8,128)} %copy.9.ids_ref, f32[32,2]{1,0:T(8,128)} %copy.10.gates_ref, f32[1,2048]{1,0:T(1,128)} %bitcast.3, bf16[1,4096,384]{2,1,0:T(8,128)(2,1)} %wg_ref.1, bf16[1,4096,384]{2,1,0:T(8,128)(2,1)} %wu_ref.1, ...), custom_call_target="tpu_custom_call" | custom-call | tf_op jit(solution)/shard_map/pallas_call | solution.py:226
  44.7 1.6 %copy.12 = bf16[32,2048]{1,0:T(8,128)(2,1)} copy(bf16[32,2048]{1,0:T(8,128)(2,1)} %shard_map.82) | data formatting | bytes 262144

commit v2 on v1

v2 whole, which is shorter than its diff:
```python
import functools

import jax
import jax.numpy as jnp
from jax import lax
from jax.experimental import pallas as pl
from jax.experimental.pallas import tpu as pltpu
from jax.sharding import PartitionSpec as P

SLOTS = 8
RMS_EPS = 1e-06
MESH = pl.DeviceIdType.MESH
F32 = jnp.float32
BF16 = jnp.bfloat16


def kernel(
    n, n_tp,
    tok_ref, gain_ref, ids_ref, gates_ref, post_ref, wg_ref, wu_ref, wd_ref,
    out_ref,
    send_buf, x_buf, wgu, wdn, h_buf, o_buf, ret_buf, stat_buf,
    w_sem, wx_send, wx_recv, d_send, d_recv, f_send, f_recv,
    h_send, h_recv, r_send, r_recv, s_send, s_recv,
):
    me = lax.axis_index("ep")
    core = lax.axis_index("tp")
    other = 1 - core
    rows, features = tok_ref.shape
    half = features // n_tp
    part = wg_ref.shape[2]
    cap = n * SLOTS

    groups = 4 if n % 4 == 0 else 1
    order = (2, 0, 3, 1) if groups == 4 else (0,)
    wide = n // groups
    plane, place = me // wide, lax.rem(me, wide)

    def target(q, r):
        return lax.rem(plane + order[q], groups) * wide + lax.rem(place + r, wide)

    def origin(q, r):
        return lax.rem(plane + groups - order[q], groups) * wide + lax.rem(place + wide - r, wide)

    def each(q, body):
        def go(r, _):
            body(q, r, q * wide + r)
            return 0

        lax.fori_loop(0 if order[q] else 1, wide, go, 0)

    own = order.index(0) * wide

    barrier = pltpu.get_barrier_semaphore()

    def greet(k, _):
        pl.semaphore_signal(barrier, inc=1, device_id={"ep": lax.rem(me + k, n)}, device_id_type=MESH)
        return 0

    lax.fori_loop(1, n, greet, 0)
    pl.semaphore_signal(barrier, inc=1, device_id={"tp": other}, device_id_type=MESH)

    own_cols = pl.ds(pl.multiple_of(core * half, half), half)
    other_cols = pl.ds(pl.multiple_of(other * half, half), half)
    own_part = pl.ds(pl.multiple_of(core * part, part), part)
    copies = [
        pltpu.make_async_copy(wg_ref.at[0], wgu.at[:, pl.ds(0, part)], w_sem.at[0]),
        pltpu.make_async_copy(wu_ref.at[0], wgu.at[:, pl.ds(part, part)], w_sem.at[1]),
        pltpu.make_async_copy(wd_ref.at[0, :, own_cols], wdn.at[own_part], w_sem.at[2]),
    ]
    for copy in copies:
        copy.start()

    ids = ids_ref[...]
    names = lax.broadcasted_iota(jnp.int32, (n, rows), 0)
    first = lax.broadcasted_iota(jnp.int32, (rows, rows), 0)
    second = lax.broadcasted_iota(jnp.int32, (rows, rows), 1)
    before = (first < second).astype(BF16)
    same = first == second
    slots = lax.broadcasted_iota(jnp.int32, (cap, rows), 0)
    count = jnp.zeros((n, 1), F32)
    picks = []
    for j in range(ids.shape[0]):
        hot = (ids[j:j + 1] == names).astype(F32)
        earlier = jnp.dot(hot.astype(BF16), before, preferred_element_type=F32) + count
        slot = jnp.sum(earlier * hot, axis=0, keepdims=True).astype(jnp.int32)
        count = count + jnp.sum(hot, axis=1, keepdims=True)
        picks.append((slots == ids[j:j + 1] * SLOTS + slot).astype(F32))

    floats = tok_ref[...].astype(F32)
    inverse = lax.rsqrt(jnp.mean(floats * floats, axis=1, keepdims=True) + RMS_EPS)
    mine = tok_ref[:, own_cols].astype(F32)
    normed = (mine * inverse * gain_ref[:, own_cols]).astype(BF16)
    dispatch = functools.reduce(lambda a, b: a + b, picks).astype(BF16)
    sent = jnp.dot(dispatch, normed, preferred_element_type=F32)
    send_buf[...] = sent.reshape(n, SLOTS, half).astype(BF16)

    pl.semaphore_wait(barrier, n)

    def to_expert(q, r, i):
        peer = target(q, r)
        return pltpu.make_async_remote_copy(
            src_ref=send_buf.at[peer], dst_ref=x_buf.at[i, core],
            send_sem=d_send.at[i], recv_sem=d_recv.at[i],
            device_id={"ep": peer}, device_id_type=MESH)

    def forward(src, block):
        return pltpu.make_async_remote_copy(
            src_ref=src, dst_ref=x_buf.at[block, core],
            send_sem=f_send.at[block], recv_sem=f_recv.at[block],
            device_id={"tp": other}, device_id_type=MESH)

    for q in range(groups):
        each(q, lambda q, r, i: to_expert(q, r, i).start())
    own_x = pltpu.make_async_copy(send_buf.at[me], x_buf.at[own, core], w_sem.at[3])
    own_x.start()
    forward(send_buf.at[me], own).start()
    down_x = pltpu.make_async_remote_copy(
        src_ref=wd_ref.at[0, :, other_cols], dst_ref=wdn.at[own_part],
        send_sem=wx_send, recv_sem=wx_recv,
        device_id={"tp": other}, device_id_type=MESH)
    down_x.start()
    own_r = pltpu.make_async_copy(o_buf.at[own], ret_buf.at[me], w_sem.at[4])

    def pass_on(q, r, i):
        to_expert(q, r, i).wait_recv()
        forward(x_buf.at[i, core], i).start()

    def give_back(q, r, i):
        peer = origin(q, r)
        return pltpu.make_async_remote_copy(
            src_ref=o_buf.at[i], dst_ref=ret_buf.at[me],
            send_sem=r_send.at[i], recv_sem=r_recv.at[me],
            device_id={"ep": peer}, device_id_type=MESH)

    def take_back(q, r, i):
        peer = target(q, r)
        return pltpu.make_async_remote_copy(
            src_ref=o_buf.at[i], dst_ref=ret_buf.at[peer],
            send_sem=r_send.at[i], recv_sem=r_recv.at[peer],
            device_id={"ep": peer}, device_id_type=MESH)

    span = max(groups // 2, 1)
    for chunk in range(groups // span):
        mine_q = range(chunk * span, (chunk + 1) * span)
        start, size = chunk * span * wide, span * wide
        for q in mine_q:
            each(q, pass_on)
        if start <= own < start + size:
            own_x.wait()

        def arrived(i, _):
            forward(x_buf.at[i, core], i).wait_recv()
            return 0

        lax.fori_loop(start, start + size, arrived, 0)
        if chunk == 0:
            for copy in copies:
                copy.wait()
        acc = jnp.zeros((size * SLOTS, 2 * part), F32)
        for side in range(n_tp):
            x = x_buf[start:start + size, side].astype(F32).reshape(size * SLOTS, half).astype(BF16)
            acc = acc + jnp.dot(x, wgu[side * half:(side + 1) * half], preferred_element_type=F32)
        gate = acc[:, :part]
        up = acc[:, part:]
        hidden = (gate / (1.0 + jnp.exp(-gate)) * up).astype(BF16)
        lines = pl.ds(start * SLOTS, size * SLOTS)
        h_buf[lines, own_part] = hidden
        hx = pltpu.make_async_remote_copy(
            src_ref=h_buf.at[lines, own_part], dst_ref=h_buf.at[lines, own_part],
            send_sem=h_send.at[chunk], recv_sem=h_recv.at[chunk],
            device_id={"tp": other}, device_id_type=MESH)
        hx.start()
        if chunk == 0:
            down_x.wait()
        hx.wait()
        result = jnp.dot(h_buf[lines], wdn[...], preferred_element_type=F32)
        o_buf[start:start + size] = result.reshape(size, SLOTS, half).astype(BF16)
        for q in mine_q:
            each(q, lambda q, r, i: give_back(q, r, i).start())
        if start <= own < start + size:
            own_r.start()

    for q in range(groups):
        each(q, lambda q, r, i: to_expert(q, r, i).wait_send())

    def passed_all(i, _):
        forward(x_buf.at[i, core], i).wait_send()
        return 0

    lax.fori_loop(0, n, passed_all, 0)
    gates = [
        jnp.sum(jnp.where(same, gates_ref[j:j + 1], 0.0), axis=1, keepdims=True)
        for j in range(ids.shape[0])
    ]
    picks = [pick.T.astype(BF16) for pick in picks]
    for q in range(groups):
        each(q, lambda q, r, i: take_back(q, r, i).wait_recv())
    own_r.wait()

    returned = ret_buf[...].astype(F32).reshape(cap, half).astype(BF16)
    combined = jnp.zeros((rows, half), F32)
    for j, pick in enumerate(picks):
        row = jnp.dot(pick, returned, preferred_element_type=F32)
        combined = combined + gates[j] * row
    low = combined.astype(BF16).astype(F32)
    squared = jnp.sum(low * low, axis=1, keepdims=True)
    stat_buf[0] = jnp.broadcast_to(squared, (rows, 128))
    sx = pltpu.make_async_remote_copy(
        src_ref=stat_buf.at[0], dst_ref=stat_buf.at[1],
        send_sem=s_send, recv_sem=s_recv,
        device_id={"tp": other}, device_id_type=MESH)
    sx.start()

    for q in range(groups):
        each(q, lambda q, r, i: give_back(q, r, i).wait_send())
    sx.wait()
    total = squared + stat_buf[1][:, 0:1]
    scale = lax.rsqrt(total / features + RMS_EPS)
    out_ref[...] = (low * scale * post_ref[...]).astype(BF16)


def shards(n, n_tp, tokens, norm_gain, expert_ids, gates, w_gate, w_up, w_down, post_gain):
    rows, features = tokens.shape
    half = features // n_tp
    part = w_gate.shape[2]
    vmem = pl.BlockSpec(memory_space=pltpu.VMEM)
    hbm = pl.BlockSpec(memory_space=pl.ANY)
    dma = pltpu.SemaphoreType.DMA
    cap = n * SLOTS
    return pl.pallas_call(
        functools.partial(kernel, n, n_tp),
        out_shape=jax.ShapeDtypeStruct((rows, half), BF16),
        in_specs=[vmem] * 5 + [hbm] * 3,
        out_specs=vmem,
        scratch_shapes=[
            pltpu.VMEM((n, SLOTS, half), BF16),
            pltpu.VMEM((n, n_tp, SLOTS, half), BF16),
            pltpu.VMEM((features, 2 * part), BF16),
            pltpu.VMEM((n_tp * part, half), BF16),
            pltpu.VMEM((cap, n_tp * part), BF16),
            pltpu.VMEM((n, SLOTS, half), BF16),
            pltpu.VMEM((n, SLOTS, half), BF16),
            pltpu.VMEM((2, rows, 128), F32),
            dma((5,)), dma, dma,
            dma((n,)), dma((n,)), dma((n,)), dma((n,)),
            dma((2,)), dma((2,)), dma((n,)), dma((n,)), dma, dma,
        ],
        compiler_params=pltpu.CompilerParams(
            collective_id=0, has_side_effects=True, vmem_limit_bytes=60 * 1024 * 1024
        ),
    )(
        tokens, norm_gain.reshape(1, -1), expert_ids.T, gates.T, post_gain.reshape(1, -1),
        w_gate, w_up, w_down,
    )


def solution(mesh):
    in_specs = (
        P("ep", None),
        P(),
        P("ep", None),
        P("ep", None),
        P("ep", None, "tp"),
        P("ep", None, "tp"),
        P("ep", "tp", None),
        P("tp"),
    )
    body = functools.partial(shards, mesh.shape["ep"], mesh.shape["tp"])
    return jax.shard_map(body, mesh=mesh, in_specs=in_specs, out_specs=P("ep", "tp"), check_vma=False)
```

time: 46.4 us -> 41.3 us (0.89)
  local copies, waits for them, and re-layouts: 4.29 us -> 1.57 us
  Pallas kernels: 41.9 us -> 39.5 us
    unnamed x3 -> x1, local copies, waits for them, and re-layouts: 4.29 us -> 1.57 us
    pallas_call x1, Pallas kernels: 41.9 us -> 39.5 us  [shards(): pl.pallas_call(functools.partial(kernel, n, n_tp), out_shape=jax.ShapeDty...]
where the time goes in v2:
time: 41.3 us; the launch traced here: 41.1 us
  Pallas kernels  39.5 us (96%)
  local copies, waits for them, and re-layouts  1.57 us (4%)
    pallas_call x1, Pallas kernels, shards(): pl.pallas_call(functools.partial(kernel, n, n_tp), out_shape=jax.ShapeDty...  39.5 us
    unnamed x1, local copies, waits for them, and re-layouts  1.57 us

profile of v2, /device:TPU:0, one launch (start us, length us, event | category | flops | bytes accessed | tf_op | source)
XLA Modules:
  0.0 41.1 jit_solution(2214652808300979488)
XLA Ops:
  0.0 39.5 %shard_map.82 = bf16[32,2048]{1,0:T(8,128)(2,1)} custom-call(bf16[32,4096]{1,0:T(8,128)(2,1)} %tok_ref.1, f32[1,4096]{1,0:T(1,128)} %bitcast.4, s32[2,32]{1,0:T(2,128)} %bitcast.6, f32[2,32]{1,0:T(2,128)} %bitcast.7, f32[1,2048]{1,0:T(1,128)} %bitcast.5, bf16[1,4096,384]{2,1,0:T(8,128)(2,1)} %wg_ref.1, bf16[1,4096,384]{2,1,0:T(8,128)(2,1)} %wu_ref.1, ...), custom_call_target="tpu_custom_call" | custom-call | tf_op jit(solution)/shard_map/pallas_call | solution.py:230
  39.6 1.6 %copy.10 = bf16[32,2048]{1,0:T(8,128)(2,1)} copy(bf16[32,2048]{1,0:T(8,128)(2,1)} %shard_map.82) | data formatting | bytes 262144

commit v3 on v2

--- a/solution.py
+++ b/solution.py
@@ -31,15 +31,19 @@
     cap = n * SLOTS
 
     groups = 4 if n % 4 == 0 else 1
-    order = (2, 0, 3, 1) if groups == 4 else (0,)
+    order = (2, 1, 3, 0) if groups == 4 else (0,)
     wide = n // groups
     plane, place = me // wide, lax.rem(me, wide)
 
+    def facing(code):
+        pair = plane + 1 - 2 * lax.rem(plane, 2)
+        return {0: plane, 1: pair, 2: lax.rem(plane + 2, 4), 3: 3 - plane}[code]
+
     def target(q, r):
-        return lax.rem(plane + order[q], groups) * wide + lax.rem(place + r, wide)
+        return facing(order[q]) * wide + lax.rem(place + r, wide)
 
     def origin(q, r):
-        return lax.rem(plane + groups - order[q], groups) * wide + lax.rem(place + wide - r, wide)
+        return facing(order[q]) * wide + lax.rem(place + wide - r, wide)
 
     def each(q, body):
         def go(r, _):

time: 41.3 us -> 39.3 us (0.952)
  Pallas kernels: 39.5 us -> 37.6 us
    pallas_call x1, Pallas kernels: 39.5 us -> 37.6 us  [shards(): pl.pallas_call(functools.partial(kernel, n, n_tp), out_shape=jax.ShapeDty...]
where the time goes in v3:
time: 39.3 us; the launch traced here: 39.2 us
  Pallas kernels  37.6 us (96%)
  local copies, waits for them, and re-layouts  1.57 us (4%)
    pallas_call x1, Pallas kernels, shards(): pl.pallas_call(functools.partial(kernel, n, n_tp), out_shape=jax.ShapeDty...  37.6 us
    unnamed x1, local copies, waits for them, and re-layouts  1.57 us

profile of v3, /device:TPU:0, one launch (start us, length us, event | category | flops | bytes accessed | tf_op | source)
XLA Modules:
  0.0 39.2 jit_solution(16154071156952663665)
XLA Ops:
  0.0 37.6 %shard_map.82 = bf16[32,2048]{1,0:T(8,128)(2,1)} custom-call(bf16[32,4096]{1,0:T(8,128)(2,1)} %tok_ref.1, f32[1,4096]{1,0:T(1,128)} %bitcast.4, s32[2,32]{1,0:T(2,128)} %bitcast.6, f32[2,32]{1,0:T(2,128)} %bitcast.7, f32[1,2048]{1,0:T(1,128)} %bitcast.5, bf16[1,4096,384]{2,1,0:T(8,128)(2,1)} %wg_ref.1, bf16[1,4096,384]{2,1,0:T(8,128)(2,1)} %wu_ref.1, ...), custom_call_target="tpu_custom_call" | custom-call | tf_op jit(solution)/shard_map/pallas_call | solution.py:234
  37.6 1.6 %copy.10 = bf16[32,2048]{1,0:T(8,128)(2,1)} copy(bf16[32,2048]{1,0:T(8,128)(2,1)} %shard_map.82) | data formatting | bytes 262144

commit v4 on v3

--- a/solution.py
+++ b/solution.py
@@ -113,7 +113,7 @@
             send_sem=f_send.at[block], recv_sem=f_recv.at[block],
             device_id={"tp": other}, device_id_type=MESH)
 
-    for q in range(groups):
+    for q in (0, 1, 3) if groups == 4 else (0,):
         each(q, lambda q, r, i: to_expert(q, r, i).start())
     own_x = pltpu.make_async_copy(send_buf.at[me], x_buf.at[own, core], w_sem.at[3])
     own_x.start()
@@ -128,6 +128,8 @@
     def pass_on(q, r, i):
         to_expert(q, r, i).wait_recv()
         forward(x_buf.at[i, core], i).start()
+        if groups == 4 and q == 0:
+            to_expert(2, r, 2 * wide + r).start()
 
     def give_back(q, r, i):
         peer = origin(q, r)

time: 39.3 us -> 39 us (level)
  Pallas kernels: 37.6 us -> 37.2 us
where the time goes in v4:
time: 39 us; the launch traced here: 38.8 us
  Pallas kernels  37.2 us (95%)
  local copies, waits for them, and re-layouts  1.57 us (4%)
    pallas_call x1, Pallas kernels, shards(): pl.pallas_call(functools.partial(kernel, n, n_tp), out_shape=jax.ShapeDty...  37.2 us
    unnamed x1, local copies, waits for them, and re-layouts  1.57 us

profile of v4, /device:TPU:0, one launch (start us, length us, event | category | flops | bytes accessed | tf_op | source)
XLA Modules:
  0.0 38.8 jit_solution(7591416996831038786)
XLA Ops:
  0.0 37.2 %shard_map.82 = bf16[32,2048]{1,0:T(8,128)(2,1)} custom-call(bf16[32,4096]{1,0:T(8,128)(2,1)} %tok_ref.1, f32[1,4096]{1,0:T(1,128)} %bitcast.4, s32[2,32]{1,0:T(2,128)} %bitcast.6, f32[2,32]{1,0:T(2,128)} %bitcast.7, f32[1,2048]{1,0:T(1,128)} %bitcast.5, bf16[1,4096,384]{2,1,0:T(8,128)(2,1)} %wg_ref.1, bf16[1,4096,384]{2,1,0:T(8,128)(2,1)} %wu_ref.1, ...), custom_call_target="tpu_custom_call" | custom-call | tf_op jit(solution)/shard_map/pallas_call | solution.py:236
  37.2 1.6 %copy.10 = bf16[32,2048]{1,0:T(8,128)(2,1)} copy(bf16[32,2048]{1,0:T(8,128)(2,1)} %shard_map.82) | data formatting | bytes 262144

commit v5 on v4

--- a/solution.py
+++ b/solution.py
@@ -47,6 +47,7 @@
 
     def each(q, body):
         def go(r, _):
+            r = (wide - 1 if order[q] else wide) - r
             body(q, r, q * wide + r)
             return 0
 

time: 39 us -> 37.8 us (0.969)
  Pallas kernels: 37.2 us -> 36.1 us
    pallas_call x1, Pallas kernels: 37.2 us -> 36.1 us  [shards(): pl.pallas_call(functools.partial(kernel, n, n_tp), out_shape=jax.ShapeDty...]
where the time goes in v5:
time: 37.8 us; the launch traced here: 37.7 us
  Pallas kernels  36.1 us (96%)
  local copies, waits for them, and re-layouts  1.57 us (4%)
    pallas_call x1, Pallas kernels, shards(): pl.pallas_call(functools.partial(kernel, n, n_tp), out_shape=jax.ShapeDty...  36.1 us
    unnamed x1, local copies, waits for them, and re-layouts  1.57 us

profile of v5, /device:TPU:0, one launch (start us, length us, event | category | flops | bytes accessed | tf_op | source)
XLA Modules:
  0.0 37.7 jit_solution(14796897719810317970)
XLA Ops:
  0.0 36.1 %shard_map.82 = bf16[32,2048]{1,0:T(8,128)(2,1)} custom-call(bf16[32,4096]{1,0:T(8,128)(2,1)} %tok_ref.1, f32[1,4096]{1,0:T(1,128)} %bitcast.4, s32[2,32]{1,0:T(2,128)} %bitcast.6, f32[2,32]{1,0:T(2,128)} %bitcast.7, f32[1,2048]{1,0:T(1,128)} %bitcast.5, bf16[1,4096,384]{2,1,0:T(8,128)(2,1)} %wg_ref.1, bf16[1,4096,384]{2,1,0:T(8,128)(2,1)} %wu_ref.1, ...), custom_call_target="tpu_custom_call" | custom-call | tf_op jit(solution)/shard_map/pallas_call | solution.py:237
  36.1 1.6 %copy.10 = bf16[32,2048]{1,0:T(8,128)(2,1)} copy(bf16[32,2048]{1,0:T(8,128)(2,1)} %shard_map.82) | data formatting | bytes 262144
